TPU v7x, 32 devices: a whole 2x2x4 slice. The times are simulated.
32 devices in a mesh: ra: 4 (over z), cb: 4 (over y, x), dp: 2 (over core).
Axes of the slice: x: 2, y: 2, z: 4, core: 2. Of those that a mesh axis runs over, the one named last changes fastest.
Arguments:
- tokens: bfloat16 [3072, 4096], P('dp', 'ra'), may hold values from -20 to 20
- pre_gain: float32 [4096], P('ra'), may hold values from 0.1 to 1.9
- up_weight: bfloat16 [4096, 16384], P('ra', 'cb'), may hold values from -0.09375 to 0.09375
- up_bias: float32 [16384], P('cb'), may hold values from -4 to 4
- down_weight: bfloat16 [16384, 4096], P('cb', 'ra'), may hold values from -0.046875 to 0.046875
- post_gain: float32 [4096], P('ra'), may hold values from 0.1 to 1.9
Outputs:
- stream_out: bfloat16 [3072, 4096], P('dp', 'ra')
All inputs are finite; a program needn't handle non-finite values.
Results may differ from a plain program's by a relative error of at most 0.0051.
Values may be sent and summed in bfloat16 or wider, within the bound.
A program may use at most 128 MiB of HBM per device.

v0:
```python
import jax
import jax.numpy as jnp
from jax import lax
from jax.sharding import PartitionSpec as P

D = 4096
epsilon = 1e-06
residual_weight = 0.5


def activate(summed, inverse, offset):
    return jnp.square(jax.nn.relu(summed * inverse[:, None] + offset)).astype(jnp.bfloat16)


def body(tokens, pre_gain, up_weight, up_bias, down_weight, post_gain):
    stream = tokens.astype(jnp.float32)
    energy = jnp.sum(stream * stream, axis=1)
    scaled = (stream * pre_gain).astype(jnp.bfloat16)
    partial_value = jnp.dot(scaled, up_weight, preferred_element_type=jnp.float32)
    total = lax.psum(energy, "ra")
    share = lax.psum_scatter(partial_value, "ra", scatter_dimension=1, tiled=True)
    width = share.shape[1]
    offset = lax.dynamic_slice_in_dim(up_bias, lax.axis_index("ra") * width, width, 0)
    hidden = activate(share, lax.rsqrt(total / D + epsilon), offset)
    branch = jnp.dot(
        lax.all_gather(hidden, "ra", axis=1, tiled=True),
        down_weight,
        preferred_element_type=jnp.float32,
    )
    branch = lax.psum(branch, "cb")
    branch_energy = lax.psum(jnp.sum(branch * branch, axis=1), "ra")
    normed = branch * lax.rsqrt(branch_energy / D + epsilon)[:, None] * post_gain
    return (residual_weight * stream + normed).astype(jnp.bfloat16)


def solution(mesh):
    in_specs = (P("dp", "ra"), P("ra"), P("ra", "cb"), P("cb"), P("cb", "ra"), P("ra"))
    out_specs = P("dp", "ra")
    return jax.shard_map(body, mesh=mesh, in_specs=in_specs, out_specs=out_specs, check_vma=False)
```

profile of v0, /device:TPU:0, one launch (start us, length us, event | category | flops | bytes accessed | tf_op | source)
XLA Modules:
  0.0 853.5 jit_solution(10800701514293128842)
XLA Ops:
  6.5 0.0 reduce-scatter.2.cloned.1.call-start
  6.5 21.1 %fusion.4 = f32[1536,4096]{1,0:T(8,128)} fusion(bf16[1024,4096]{1,0:T(8,128)(2,1)} %param.8, bf16[1536,1024]{1,0:T(8,128)(2,1)} %param.6, f32[1024]{0:T(1024)} %param.7), kind=kOutput, calls=%fused_computation.9 | convolution fusion | flops 12889620480 | bytes 36704256 | tf_op jit(solution)/shard_map/dot_general | solution.py:19
  27.7 0.0 copy-start
  27.7 0.0 reduce-scatter.2.cloned.1.call-update
  27.7 0.0 all-gather.2.cloned.1.call-start
  27.8 0.8 dynamic_slice.3
  28.6 1.0 copy-done
  29.6 0.7 fusion.3
  30.3 14.3 %psum.21 = f32[1536]{0:T(1024)S(1)} all-reduce(f32[1536]{0:T(1024)S(1)} %fusion.3), channel_id=1, replica_groups=mesh['ra'=4,'cb'=4,'dp'=2] {'ra'}, use_global_device_ids=true, to_apply=%region_2.0 | all-reduce | flops 1536 | bytes 12288 | tf_op jit(solution)/shard_map/psum | solution.py:20
  44.6 400.5 %reduce-scatter.2.cloned.1.call-done = f32[1536,1024]{1,0:T(8,128)} async-done(((f32[1536,4096]{1,0:T(8,128)}), f32[1536,1024]{1,0:T(8,128)}) %reduce-scatter.2.cloned.1.call-update) | async-done | bytes 6291472 | tf_op jit(solution)/shard_map/reduce_scatter | solution.py:21
  445.2 5.4 multiply_convert_fusion
  450.6 0.0 all-gather.2.cloned.1.call-update
  450.6 0.0 all-reduce.2.cloned.1.call-start
  450.7 220.3 %all-gather.2.cloned.1.call-done = bf16[1536,4096]{1,0:T(8,128)(2,1)} async-done(((bf16[1536,1024]{1,0:T(8,128)(2,1)}), bf16[1536,4096]{1,0:T(8,128)(2,1)}) %all-gather.2.cloned.1.call-update) | async-done | bytes 12582928 | tf_op jit(solution)/shard_map/all_gather | solution.py:26
  671.0 19.5 %fusion.7 = f32[1536,1024]{1,0:T(8,128)} fusion(bf16[1536,4096]{1,0:T(8,128)(2,1)} %all-gather.2.cloned.1.call-done, bf16[4096,1024]{1,0:T(8,128)(2,1)} %param.10), kind=kOutput, calls=%fused_computation.13 | convolution fusion | flops 12884901888 | bytes 27262976 | tf_op jit(solution)/shard_map/dot_general | solution.py:25
  690.5 0.0 copy-start.1
  690.5 0.0 all-reduce.2.cloned.1.call-update
  690.5 136.5 %all-reduce.2.cloned.1.call-done = f32[1536,1024]{1,0:T(8,128)} async-done(((f32[1536,1024]{1,0:T(8,128)}), f32[1536,1024]{1,0:T(8,128)}) %all-reduce.2.cloned.1.call-update) | async-done | bytes 6291472 | tf_op jit(solution)/shard_map/psum | solution.py:30
  827.0 3.3 multiply_reduce_fusion
  830.3 11.9 %psum.23 = f32[1536]{0:T(1024)S(1)} all-reduce(f32[1536]{0:T(1024)S(1)} %multiply_reduce_fusion), channel_id=1, replica_groups=mesh['ra'=4,'cb'=4,'dp'=2] {'ra'}, use_global_device_ids=true, to_apply=%region_5.6 | all-reduce | flops 1536 | bytes 12288 | tf_op jit(solution)/shard_map/psum | solution.py:31
  842.3 0.0 copy-done.1
  842.3 4.7 fusion.1
  (2 shorter events, 0.0 us)
Async XLA Ops:
  6.5 438.6 %reduce-scatter.2.cloned.1.call-start = ((), (), s32[]{:S(2)}) async-start(), calls=%async_computation.1 | async-start | bytes 31457280 | tf_op jit(solution)/shard_map/reduce_scatter | solution.py:21
  27.7 1.9 copy-start
  27.7 643.3 %all-gather.2.cloned.1.call-start = ((), (), s32[]{:S(2)}) async-start(), calls=%async_computation.2 | async-start | bytes 15728640 | tf_op jit(solution)/shard_map/all_gather | solution.py:26
  450.6 376.4 %all-reduce.2.cloned.1.call-start = ((), (), s32[]{:S(2)}) async-start(), calls=%async_computation.3 | async-start | bytes 12582912 | tf_op jit(solution)/shard_map/psum | solution.py:30
  690.5 151.8 %copy-start.1 = (f32[1024]{0:T(1024)S(1)}, f32[1024]{0:T(1024)}, u32[]{:S(2)}) copy-start(f32[1024]{0:T(1024)} %param.11) | copy-start | bytes 12292
Sparse Core Ops, SparseCore 0:
  27.8 417.2 reduce-scatter.1
  450.7 220.2 all-gather.1
  690.6 136.3 all-reduce.1
where the time goes:
time: 854 us
  waiting for transfers between devices  757 us (89%)
  matrix products  40.6 us (5%)
  blocking collectives  26.3 us (3%)
  other arithmetic  14.1 us (2%)
  between operations  13.2 us (2%)
    reduce_scatter x1, waiting for transfers between devices, body(): lax.psum_scatter(partial_value, 'ra', scatter_dimension=1, tiled=True)  401 us
    all_gather x1, waiting for transfers between devices, body(): lax.all_gather(hidden, 'ra', axis=1, tiled=True)  220 us
    psum x1, waiting for transfers between devices, body(): branch = lax.psum(branch, 'cb')  137 us
    dot_general x1, matrix products, body(): jnp.dot(scaled, up_weight, preferred_element_type=jnp.float32)  21.1 us
    dot_general x1, matrix products, body(): jnp.dot(lax.all_gather(hidden, 'ra', axis=1, tiled=True), down_weight, pr...  19.5 us
  transfers between devices with their start and end apart: 3, of which 3 were waited for; matrix products, arithmetic and copies ran while one was open for 0% of the time, Pallas kernels for 0%

commit v1 on v0

--- a/solution.py
+++ b/solution.py
@@ -6,6 +6,10 @@
 D = 4096
 epsilon = 1e-06
 residual_weight = 0.5
+
+
+def pass_teams_for(arr_in):
+    return lax.all_gather(arr_in, axis_name="cb").sum(axis=0)
 
 
 def activate(summed, inverse, offset):
@@ -27,7 +31,7 @@
         down_weight,
         preferred_element_type=jnp.float32,
     )
-    branch = lax.psum(branch, "cb")
+    branch = pass_teams_for(branch)
     branch_energy = lax.psum(jnp.sum(branch * branch, axis=1), "ra")
     normed = branch * lax.rsqrt(branch_energy / D + epsilon)[:, None] * post_gain
     return (residual_weight * stream + normed).astype(jnp.bfloat16)

time: 854 us -> 956 us (1.12)
  waiting for transfers between devices: 757 us -> 847 us
  other arithmetic: 14.1 us -> 27 us
    all_gather x0 -> x1, waiting for transfers between devices: none -> 226 us  [pass_teams_for(): return lax.all_gather(arr_in, axis_name='cb').sum(axis=0)]
    psum x1 -> x0, waiting for transfers between devices: 137 us -> none  [body(): branch = lax.psum(branch, 'cb')]
    reduce_sum x0 -> x1, other arithmetic: none -> 12.9 us  [pass_teams_for(): return lax.all_gather(arr_in, axis_name='cb').sum(axis=0)]
where the time goes in v1:
time: 956 us
  waiting for transfers between devices  847 us (89%)
  matrix products  40.7 us (4%)
  other arithmetic  27 us (3%)
  blocking collectives  26.3 us (3%)
  between operations  13.2 us (1%)
    reduce_scatter x1, waiting for transfers between devices, body(): lax.psum_scatter(partial_value, 'ra', scatter_dimension=1, tiled=True)  401 us
    all_gather x1, waiting for transfers between devices, pass_teams_for(): return lax.all_gather(arr_in, axis_name='cb').sum(axis=0)  226 us
    all_gather x1, waiting for transfers between devices, body(): lax.all_gather(hidden, 'ra', axis=1, tiled=True)  220 us
    dot_general x1, matrix products, body(): jnp.dot(scaled, up_weight, preferred_element_type=jnp.float32)  21.1 us
    dot_general x1, matrix products, body(): jnp.dot(lax.all_gather(hidden, 'ra', axis=1, tiled=True), down_weight, pr...  19.5 us
  transfers between devices with their start and end apart: 3, of which 3 were waited for; matrix products, arithmetic and copies ran while one was open for 0% of the time, Pallas kernels for 0%

profile of v1, /device:TPU:0, one launch (start us, length us, event | category | flops | bytes accessed | tf_op | source)
XLA Modules:
  0.0 955.9 jit_solution(27130960487670077)
XLA Ops:
  6.5 0.0 reduce-scatter.2.cloned.1.call-start
  6.5 21.1 %fusion.4 = f32[1536,4096]{1,0:T(8,128)} fusion(bf16[1024,4096]{1,0:T(8,128)(2,1)} %param.8, bf16[1536,1024]{1,0:T(8,128)(2,1)} %param.6, f32[1024]{0:T(1024)} %param.7), kind=kOutput, calls=%fused_computation.9 | convolution fusion | flops 12889620480 | bytes 36704256 | tf_op jit(solution)/shard_map/dot_general | solution.py:23
  27.7 0.0 copy-start
  27.7 0.0 reduce-scatter.2.cloned.1.call-update
  27.7 0.0 all-gather.4.cloned.1.call-start
  27.8 0.8 dynamic_slice.3
  28.6 1.0 copy-done
  29.6 0.7 fusion.3
  30.3 14.4 %psum.14 = f32[1536]{0:T(1024)S(1)} all-reduce(f32[1536]{0:T(1024)S(1)} %fusion.3), channel_id=1, replica_groups=mesh['ra'=4,'cb'=4,'dp'=2] {'ra'}, use_global_device_ids=true, to_apply=%region_2.0 | all-reduce | flops 1536 | bytes 12288 | tf_op jit(solution)/shard_map/psum | solution.py:24
  44.7 400.5 %reduce-scatter.2.cloned.1.call-done = f32[1536,1024]{1,0:T(8,128)} async-done(((f32[1536,4096]{1,0:T(8,128)}), f32[1536,1024]{1,0:T(8,128)}) %reduce-scatter.2.cloned.1.call-update) | async-done | bytes 6291472 | tf_op jit(solution)/shard_map/reduce_scatter | solution.py:25
  445.2 5.4 multiply_convert_fusion
  450.6 0.0 all-gather.4.cloned.1.call-update
  450.6 0.2 all-gather.6.cloned.1.call-start
  450.9 220.2 %all-gather.4.cloned.1.call-done = bf16[1536,4096]{1,0:T(8,128)(2,1)} async-done(((bf16[1536,1024]{1,0:T(8,128)(2,1)}), bf16[1536,4096]{1,0:T(8,128)(2,1)}) %all-gather.4.cloned.1.call-update) | async-done | bytes 12582928 | tf_op jit(solution)/shard_map/all_gather | solution.py:30
  671.0 19.5 %fusion.7 = f32[1536,1024]{1,0:T(8,128)} fusion(bf16[1536,4096]{1,0:T(8,128)(2,1)} %all-gather.4.cloned.1.call-done, bf16[4096,1024]{1,0:T(8,128)(2,1)} %param.10), kind=kOutput, calls=%fused_computation.13 | convolution fusion | flops 12884901888 | bytes 27262976 | tf_op jit(solution)/shard_map/dot_general | solution.py:29
  690.5 0.0 all-gather.6.cloned.1.call-update
  690.5 225.9 %all-gather.6.cloned.1.call-done = f32[6144,1024]{1,0:T(8,128)} async-done(((f32[1536,1024]{1,0:T(8,128)}), f32[6144,1024]{1,0:T(8,128)}) %all-gather.6.cloned.1.call-update) | async-done | bytes 25165840 | tf_op jit(solution)/shard_map/all_gather | solution.py:12
  916.5 12.9 %reduce_sum.28 = f32[1536,1024]{1,0:T(8,128)} reduce(f32[4,1536,1024]{2,1,0:T(8,128)} %bitcast.4, f32[]{:T(128)} %constant.9.clone.1), dimensions={0}, to_apply=%region_3.4 | reduce | flops 4718592 | bytes 31457284 | tf_op jit(solution)/shard_map/reduce_sum | solution.py:12
  929.4 0.0 copy-start.1
  929.4 3.3 multiply_reduce_fusion
  932.6 11.9 %psum.15 = f32[1536]{0:T(1024)S(1)} all-reduce(f32[1536]{0:T(1024)S(1)} %multiply_reduce_fusion), channel_id=1, replica_groups=mesh['ra'=4,'cb'=4,'dp'=2] {'ra'}, use_global_device_ids=true, to_apply=%region_5.6 | all-reduce | flops 1536 | bytes 12288 | tf_op jit(solution)/shard_map/psum | solution.py:35
  944.6 0.0 copy-done.1
  944.6 4.7 fusion.1
  (2 shorter events, 0.0 us)
Async XLA Ops:
  6.5 438.6 %reduce-scatter.2.cloned.1.call-start = ((), (), s32[]{:S(2)}) async-start(), calls=%async_computation.1 | async-start | bytes 31457280 | tf_op jit(solution)/shard_map/reduce_scatter | solution.py:25
  27.7 1.9 copy-start
  27.7 643.3 %all-gather.4.cloned.1.call-start = ((), (), s32[]{:S(2)}) async-start(), calls=%async_computation.2 | async-start | bytes 15728640 | tf_op jit(solution)/shard_map/all_gather | solution.py:30
  450.6 465.8 %all-gather.6.cloned.1.call-start = ((), (), s32[]{:S(2)}) async-start(), calls=%async_computation.3 | async-start | bytes 31457280 | tf_op jit(solution)/shard_map/all_gather | solution.py:12
  929.4 15.2 %copy-start.1 = (f32[1024]{0:T(1024)S(1)}, f32[1024]{0:T(1024)}, u32[]{:S(2)}) copy-start(f32[1024]{0:T(1024)} %param.11) | copy-start | bytes 12292
Sparse Core Ops, SparseCore 0:
  27.8 417.2 reduce-scatter.1
  450.7 220.2 all-gather.3
  690.7 225.7 all-gather.5
